TPU v7x, 32 devices: a whole 2x2x4 slice. The times are simulated.
32 devices in a mesh: grp: 2 (over x), ep: 16 (over z, y, core).
Axes of the slice: x: 2, y: 2, z: 4, core: 2. Of those that a mesh axis runs over, the one named last changes fastest.
Arguments:
- residual: bfloat16 [16, 4096], P('grp', 'ep'), parts along dimension 0, may hold values from -6 to 6
- head_states: float32 [64, 512, 1024], P(('grp', 'ep')), parts along dimension 0, may hold values from -6 to 6
- first_gain: bfloat16 [4096], replicated, may hold values from 0.099609375 to 1.8984375
- w_query: bfloat16 [4096, 2048], P(None, 'ep'), may hold values from -0.09375 to 0.09375
- w_key: bfloat16 [4096, 2048], P(None, 'ep'), may hold values from -0.09375 to 0.09375
- w_value: bfloat16 [4096, 4096], P(None, 'ep'), may hold values from -0.09375 to 0.09375
- w_gate: bfloat16 [4096, 4096], P(None, 'ep'), may hold values from -0.09375 to 0.09375
- w_low: bfloat16 [4096, 16], replicated, may hold values from -0.09375 to 0.09375
- w_decay: bfloat16 [16, 2048], replicated, may hold values from -15 to 15
- decay_bias: float32 [2048], replicated, may hold values from -40 to 4
- head_gain: bfloat16 [1024], replicated, may hold values from 0.099609375 to 1.8984375
- w_output: bfloat16 [4096, 4096], P(None, 'ep'), may hold values from -0.09375 to 0.09375
- second_gain: bfloat16 [4096], replicated, may hold values from 0.099609375 to 1.8984375
- routes: int32 [16, 2], P('grp'), parts along dimension 0, may hold values from 0 to 15, as said below
- group_logits: float32 [16, 4], P('grp'), parts along dimension 0, may hold values from -12 to 12
- expert_logits: float32 [16, 2], P('grp'), parts along dimension 0, may hold values from -9 to 9
- expert_gate: bfloat16 [16, 4096, 512], P('ep'), may hold values from -0.09375 to 0.09375
- expert_up: bfloat16 [16, 4096, 512], P('ep'), may hold values from -0.09375 to 0.09375
- expert_down: bfloat16 [16, 512, 4096], P('ep'), may hold values from -0.25 to 0.25
Outputs:
- layer_out: bfloat16 [16, 4096], P('grp', 'ep'), parts along dimension 0
- new_states: float32 [64, 512, 1024], P(('grp', 'ep')), parts along dimension 0
There are 2 independent parts, one for each index of `grp`. A program takes and returns all parts, laid end to end along the dimension named above; an argument that names none is the same for every part. Nothing has to cross between parts.
Inputs may be any that keep to these rules, and one draw needn't show every extreme that they name: `routes`: each row names 2 different experts of one group (numbers g * 4 to g * 4 + 3). No expert is named by more than 2 rows, and in every draw all experts of one group are named by exactly 2 rows.
All inputs are finite; a program needn't handle non-finite values.
Results may differ from a plain program's by a relative error of at most 0.014.
Values may be sent and summed in bfloat16 or wider, within the bound.
No kernel may reach another device: no remote copies, remote signals or barrier semaphores. Data moves between devices by JAX's collectives and lax.ppermute only.
A program may use at most 128 MiB of HBM per device.

v0:
```python
import jax
import jax.numpy as jnp
import numpy as np
from jax import lax
from jax.sharding import PartitionSpec as P

HEADS = 4
DK = 512
DV = 1024
GROUPS = 4
TOP = 2
norm_eps = 1e-06
decay_tau = 16.0


def rms_scale(values, gain):
    floats = values.astype(jnp.float32)
    return (
        floats
        * lax.rsqrt(jnp.mean(floats * floats, axis=-1, keepdims=True) + norm_eps)
        * gain.astype(jnp.float32)
    )


def route_weights(routes, group_logits, expert_logits, per_group):
    group_exp = jnp.exp(group_logits)
    group_prob = group_exp / jnp.sum(group_exp, axis=1, keepdims=True)
    chosen = routes[:, 0] // per_group
    groups_row = jnp.arange(group_logits.shape[1], dtype=jnp.int32)
    picked = jnp.sum(
        group_prob * (chosen[:, None] == groups_row[None, :]).astype(jnp.float32), axis=1
    )
    expert_exp = jnp.exp(expert_logits)
    return expert_exp / jnp.sum(expert_exp, axis=1, keepdims=True) * picked[:, None]


def per_device(
    residual,
    head_states,
    first_gain,
    w_query,
    w_key,
    w_value,
    w_gate,
    w_low,
    w_decay,
    decay_bias,
    head_gain,
    w_output,
    second_gain,
    routes,
    group_logits,
    expert_logits,
    expert_gate,
    expert_up,
    expert_down,
):
    devices = lax.axis_size("ep")
    my_index = lax.axis_index("ep")
    seq_count = residual.shape[0]
    own_width = residual.shape[1]
    width = own_width * devices
    pairs_dev = head_states.shape[0]
    slot_count = max(1, pairs_dev // HEADS)
    rows = lax.all_gather(residual, "ep", axis=1, tiled=True)
    normed = rms_scale(rows, first_gain).astype(jnp.bfloat16)
    my_head = my_index * HEADS // devices
    target = jnp.arange(devices, dtype=jnp.int32)[:, None]
    turn = jnp.arange(slot_count, dtype=jnp.int32)[None, :]
    within = jnp.mod(my_head - target * pairs_dev, HEADS) + turn * HEADS
    target_seq = (target * pairs_dev + within) // HEADS
    seq_row = jnp.arange(seq_count, dtype=jnp.int32)[None, None, :]
    picker = (target_seq[:, :, None] == seq_row) & (within < pairs_dev)[:, :, None]
    picker = picker.astype(jnp.bfloat16).reshape(devices * slot_count, seq_count)

    def outgoing(weight):
        projected = jnp.dot(normed, weight, preferred_element_type=jnp.float32).astype(jnp.bfloat16)
        placed = jnp.dot(picker, projected, preferred_element_type=jnp.float32).astype(jnp.bfloat16)
        return placed.reshape(devices, slot_count, projected.shape[1])

    send_query = outgoing(w_query)
    send_key = outgoing(w_key)
    send_value = outgoing(w_value)
    send_gate = outgoing(w_gate)
    incoming = (
        lax.all_to_all(send_query, "ep", split_axis=0, concat_axis=0, tiled=True),
        lax.all_to_all(send_key, "ep", split_axis=0, concat_axis=0, tiled=True),
        lax.all_to_all(send_value, "ep", split_axis=0, concat_axis=0, tiled=True),
        lax.all_to_all(send_gate, "ep", split_axis=0, concat_axis=0, tiled=True),
    )
    pair_ids = my_index * pairs_dev + jnp.arange(pairs_dev, dtype=jnp.int32)
    head_pick = (
        jnp.mod(pair_ids, HEADS)[:, None] == jnp.arange(HEADS, dtype=jnp.int32)[None, :]
    ).astype(jnp.bfloat16)
    turns = np.arange(pairs_dev) // HEADS
    pair_rows = np.arange(pairs_dev)

    def arrange(received):
        merged = jnp.dot(head_pick, received.reshape(HEADS, -1), preferred_element_type=jnp.float32)
        merged = merged.reshape(pairs_dev, devices // HEADS, slot_count, received.shape[2])
        return merged[pair_rows, :, turns, :].reshape(pairs_dev, -1).astype(jnp.bfloat16)

    query = arrange(incoming[0])
    key = arrange(incoming[1])
    value = arrange(incoming[2])
    gate = arrange(incoming[3])
    low = jnp.dot(normed, w_low, preferred_element_type=jnp.float32)
    decay_pre = (
        jnp.dot(low, w_decay.astype(jnp.float32), precision=lax.Precision.HIGHEST) + decay_bias
    )
    decay_pre = lax.dynamic_slice_in_dim(
        decay_pre.reshape(seq_count * HEADS, DK), my_index * pairs_dev, pairs_dev, 0
    )
    log_decay = jax.nn.log_sigmoid(decay_pre) / decay_tau
    new_states = (
        head_states * jnp.exp(log_decay)[:, :, None]
        + key.astype(jnp.float32)[:, :, None] * value.astype(jnp.float32)[:, None, :]
    )
    read = jnp.einsum(
        "pk,pkv->pv",
        query.astype(jnp.float32) * DK ** (-0.5),
        new_states,
        precision=lax.Precision.HIGHEST,
    )
    mixed = (rms_scale(read, head_gain) * jax.nn.silu(gate.astype(jnp.float32))).astype(
        jnp.bfloat16
    )
    gathered = lax.all_gather(mixed, "ep", axis=0, tiled=True).reshape(seq_count, HEADS * DV)
    branch = jnp.dot(gathered, w_output, preferred_element_type=jnp.float32).astype(jnp.bfloat16)
    stream = (residual.astype(jnp.float32) + branch.astype(jnp.float32)).astype(jnp.bfloat16)
    floats = stream.astype(jnp.float32)
    total = lax.psum(jnp.sum(floats * floats, axis=1), "ep")
    gain_part = lax.dynamic_slice_in_dim(second_gain, my_index * own_width, own_width)
    scaled = floats * lax.rsqrt(total / width + norm_eps)[:, None] * gain_part.astype(jnp.float32)
    expert_in = lax.all_gather(scaled.astype(jnp.bfloat16), "ep", axis=1, tiled=True)
    capacity = 2 * seq_count * TOP // devices
    weights = route_weights(routes, group_logits, expert_logits, devices // GROUPS)
    hits = (routes == my_index).astype(jnp.int32)
    mine = jnp.sum(weights * hits.astype(jnp.float32), axis=1)
    routed = jnp.sum(hits, axis=1)
    slot = jnp.cumsum(routed) - routed
    chooser = (slot[None, :] == jnp.arange(capacity, dtype=jnp.int32)[:, None]) & (
        routed[None, :] > 0
    )
    picked = jnp.dot(
        chooser.astype(jnp.bfloat16), expert_in, preferred_element_type=jnp.float32
    ).astype(jnp.bfloat16)
    row_weight = jnp.dot(chooser.astype(jnp.float32), mine, precision=lax.Precision.HIGHEST)
    gate_part = jnp.dot(picked, expert_gate[0], preferred_element_type=jnp.float32)
    up_part = jnp.dot(picked, expert_up[0], preferred_element_type=jnp.float32)
    active = (jax.nn.silu(gate_part) * up_part * row_weight[:, None]).astype(jnp.bfloat16)
    expert_rows = jnp.dot(active, expert_down[0], preferred_element_type=jnp.float32).astype(
        jnp.bfloat16
    )
    arrived = lax.all_to_all(expert_rows, "ep", split_axis=1, concat_axis=0, tiled=True)
    every = jnp.arange(devices, dtype=jnp.int32)
    hit_all = jnp.sum((routes[:, :, None] == every[None, None, :]).astype(jnp.int32), axis=1)
    slot_all = jnp.cumsum(hit_all, axis=0) - hit_all
    placer = (slot_all[:, :, None] == jnp.arange(capacity, dtype=jnp.int32)[None, None, :]) & (
        hit_all[:, :, None] > 0
    )
    placer = placer.astype(jnp.bfloat16).reshape(seq_count, devices * capacity)
    returned = jnp.dot(placer, arrived, preferred_element_type=jnp.float32)
    layer_out = (stream.astype(jnp.float32) + returned).astype(jnp.bfloat16)
    return (layer_out, new_states)


def solution(mesh):
    return jax.shard_map(
        per_device,
        mesh=mesh,
        in_specs=(
            P("grp", "ep"),
            P(("grp", "ep"), None, None),
            P(),
            P(None, "ep"),
            P(None, "ep"),
            P(None, "ep"),
            P(None, "ep"),
            P(),
            P(),
            P(),
            P(),
            P(None, "ep"),
            P(),
            P("grp", None),
            P("grp", None),
            P("grp", None),
            P("ep", None, None),
            P("ep", None, None),
            P("ep", None, None),
        ),
        out_specs=(P("grp", "ep"), P(("grp", "ep"), None, None)),
        check_vma=False,
    )
```

profile of v0, /device:TPU:0, one launch (start us, length us, event | category | flops | bytes accessed | tf_op | source)
XLA Modules:
  0.0 169.2 jit_solution(12246803465482614124)
XLA Ops:
  0.6 0.0 copy-start
  0.6 0.0 copy-start.3
  0.7 0.0 copy-start.4
  0.7 0.0 copy-start.6
  0.7 0.0 copy-start.5
  0.7 23.7 %all_gather.9 = bf16[8,4096]{1,0:T(8,128)(2,1)S(1)} all-gather(bf16[8,256]{1,0:T(8,128)(2,1)} %param.29), channel_id=1, replica_groups=mesh['grp'=2,'ep'=16] {'ep'}, dimensions={1}, use_global_device_ids=true | all-gather | bytes 69632 | tf_op jit(solution)/shard_map/all_gather | solution.py:65
  24.4 0.1 fusion.26
  24.6 0.7 convert_element_type.145
  25.3 1.6 fusion.14
  26.9 0.6 copy.61
  27.5 3.4 %all-to-all-start.1 = ((bf16[16,1,128]{2,1,0:T(2,128)(2,1)}), bf16[16,1,128]{2,1,0:T(2,128)(2,1)S(1)}, u32[]{:S(2)}, u32[]{:S(2)}) async-start(bf16[16,1,128]{2,1,0:T(2,128)(2,1)} %copy.61), calls=%async_computation.1 | async-start | bytes 16384 | tf_op jit(solution)/shard_map/all_to_all | solution.py:87
  31.0 0.7 fusion.70
  31.7 0.7 fusion.73
  32.4 0.8 convert_reduce_fusion
  33.1 0.5 fusion.5
  33.6 1.1 fusion.88
  34.8 1.0 convolution_add_fusion
  35.8 1.6 fusion.13
  37.4 2.1 %fusion.6 = bf16[16,1,256]{2,0,1:T(8,128)(2,1)S(1)} fusion(bf16[4096,256]{1,0:T(8,128)(2,1)} %param.35, s32[16]{0:T(128)S(1)} %and_select_fusion.1, pred[16]{0:T(512)(128)(4,1)S(1)} %broadcast_compare_fusion.2, bf16[8,4096]{1,0:T(8,128)(2,1)S(1)} %all_gather.9, f32[4096]{0:T(1024)S(1)} %convert_element_type.145, f32[8]{0:T(128)S(1)} %add_rsqrt_fusion.2), kind=kOutput, calls=%fused_computation.16 | convolution fusion | flops 16980224 | bytes 2187376 | tf_op jit(solution)/shard_map/dot_general | solution.py:78
  39.6 0.2 reduce-window.8
  39.9 0.8 dynamic-slice_convert_fusion
  40.7 0.1 convolution_bitcast_fusion.5
  40.8 0.5 broadcast.372
  41.3 0.6 reduce.5
  42.0 0.6 reshape.330
  42.6 0.6 copy.59
  43.2 0.6 reduce.4
  43.9 0.6 reshape.328
  44.5 0.0 copy-done.5
  44.5 0.0 all-to-all-done.1
  44.5 6.0 %all-to-all-start = ((bf16[16,1,128]{2,1,0:T(2,128)(2,1)}), bf16[16,1,128]{2,1,0:T(2,128)(2,1)S(1)}, u32[]{:S(2)}, u32[]{:S(2)}) async-start(bf16[16,1,128]{2,1,0:T(2,128)(2,1)} %copy.59), calls=%async_computation | async-start | bytes 16384 | tf_op jit(solution)/shard_map/all_to_all | solution.py:86
  50.5 0.2 convolution_bitcast_fusion.3
  50.7 0.6 gather_fusion.1
  51.3 5.5 %all-to-all-done = bf16[16,1,128]{2,1,0:T(2,128)(2,1)S(1)} async-done(((bf16[16,1,128]{2,1,0:T(2,128)(2,1)}), bf16[16,1,128]{2,1,0:T(2,128)(2,1)S(1)}, u32[]{:S(2)}, u32[]{:S(2)}) %all-to-all-start) | async-done | bytes 4128 | tf_op jit(solution)/shard_map/all_to_all | solution.py:86
  56.8 3.4 %all-to-all-start.2 = ((bf16[16,2,128]{2,1,0:T(2,128)(2,1)}), bf16[16,2,128]{2,1,0:T(2,128)(2,1)S(1)}, u32[]{:S(2)}, u32[]{:S(2)}) async-start(bf16[16,2,128]{2,1,0:T(2,128)(2,1)} %reshape.330), calls=%async_computation.2 | async-start | bytes 16384 | tf_op jit(solution)/shard_map/all_to_all | solution.py:88
  60.3 0.2 convolution_bitcast_fusion.4
  60.5 0.6 gather_fusion
  61.1 5.6 %all-to-all-done.2 = bf16[16,2,128]{2,1,0:T(2,128)(2,1)S(1)} async-done(((bf16[16,2,128]{2,1,0:T(2,128)(2,1)}), bf16[16,2,128]{2,1,0:T(2,128)(2,1)S(1)}, u32[]{:S(2)}, u32[]{:S(2)}) %all-to-all-start.2) | async-done | bytes 8224 | tf_op jit(solution)/shard_map/all_to_all | solution.py:88
  66.6 3.5 %all-to-all-start.3 = ((bf16[16,2,128]{2,1,0:T(2,128)(2,1)}), bf16[16,2,128]{2,1,0:T(2,128)(2,1)S(1)}, u32[]{:S(2)}, u32[]{:S(2)}) async-start(bf16[16,2,128]{2,1,0:T(2,128)(2,1)} %reshape.328), calls=%async_computation.3 | async-start | bytes 16384 | tf_op jit(solution)/shard_map/all_to_all | solution.py:89
  70.1 0.1 reduce.2
  70.2 0.2 convolution_bitcast_fusion.2
  70.4 0.6 gather_fusion.2
  71.0 2.7 %multiply_add_fusion = f32[2,512,1024]{2,1,0:T(8,128)S(1)} fusion(f32[2,512,1024]{2,1,0:T(8,128)} %param.30, f32[2,1024]{1,0:T(2,128)S(1)} %bitcast.122, f32[2,512]{1,0:T(2,128)S(1)} %bitcast.124, f32[2,512]{1,0:T(2,128)S(1)} %fusion.44), kind=kLoop, calls=%fused_computation.11 | loop fusion | flops 3145728 | bytes 8404992 | tf_op jit(solution)/shard_map/add | solution.py:116
  73.7 0.0 copy-start.1
  73.8 0.0 copy-start.2
  73.8 2.0 %copy-done.1 = f32[2,512,1024]{2,1,0:T(8,128)} copy-done((f32[2,512,1024]{2,1,0:T(8,128)}, f32[2,512,1024]{2,1,0:T(8,128)S(1)}, u32[]{:S(2)}) %copy-start.1) | copy-done | bytes 4194328
  75.8 2.1 %fusion.92 = f32[2,1,1024]{2,1,0:T(1,128)S(1)} fusion(f32[2,512,1]{1,2,0:T(1,128)S(1)} %bitcast.123, f32[2,512,1024]{2,1,0:T(8,128)S(1)} %multiply_add_fusion), kind=kOutput, calls=%fused_computation.142 | convolution fusion | flops 12582912 | bytes 4206592 | tf_op jit(solution)/shard_map/pk,pkv->pv/dot_general | solution.py:119
  77.8 0.1 fusion.32
  78.0 0.0 all-to-all-done.3
  78.0 0.1 reduce.3
  78.1 0.2 convolution_bitcast_fusion.1
  78.3 0.6 gather_fusion.3
  78.9 0.1 fusion.60
  78.9 21.8 %all-gather = bf16[16,2,1024]{2,1,0:T(2,128)(2,1)S(1)} all-gather(bf16[1,2,1024]{2,1,0:T(2,128)(2,1)S(1)} %fusion.60), channel_id=1, replica_groups=mesh['grp'=2,'ep'=16] {'ep'}, dimensions={0}, use_global_device_ids=true | all-gather | bytes 69632 | tf_op jit(solution)/shard_map/all_gather | solution.py:128
  100.8 2.1 %multiply_reduce_fusion = (f32[8]{0:T(128)S(1)}, f32[8,256]{1,0:T(8,128)S(1)}) fusion(bf16[8,4096]{1,0:T(8,128)(2,1)S(1)} %reshape.284, bf16[4096,256]{1,0:T(8,128)(2,1)} %param.40, bf16[8,256]{1,0:T(8,128)(2,1)S(1)} %copy-done.2), kind=kOutput, calls=%fused_computation.58 | convolution fusion | flops 16793592 | bytes 2175008 | tf_op jit(solution)/shard_map/dot_general | solution.py:129
  102.9 29.8 %psum.7 = f32[8]{0:T(128)S(1)} all-reduce(f32[8]{0:T(128)S(1)} %get-tuple-element.2), channel_id=1, replica_groups=mesh['grp'=2,'ep'=16] {'ep'}, use_global_device_ids=true, to_apply=%region_7.8 | all-reduce | flops 8 | bytes 64 | tf_op jit(solution)/shard_map/psum | solution.py:132
  132.7 0.1 multiply_convert_fusion
  132.8 17.3 %all_gather.11 = bf16[8,4096]{1,0:T(8,128)(2,1)S(1)} all-gather(bf16[8,256]{1,0:T(8,128)(2,1)S(1)} %multiply_convert_fusion), channel_id=1, replica_groups=mesh['grp'=2,'ep'=16] {'ep'}, dimensions={1}, use_global_device_ids=true | all-gather | bytes 69632 | tf_op jit(solution)/shard_map/all_gather | solution.py:135
  150.1 0.1 convolution_convert_fusion.1
  150.2 2.8 %fusion.3 = f32[2,512]{1,0:T(2,128)S(1)} fusion(bf16[2,4096]{1,0:T(2,128)(2,1)S(1)} %convolution_convert_fusion.1, bf16[1,4096,512]{2,1,0:T(8,128)(2,1)} %param.45), kind=kOutput, calls=%fused_computation.9 | convolution fusion | flops 8388608 | bytes 4214784 | tf_op jit(solution)/shard_map/dot_general | solution.py:149
  153.1 5.4 %convolution_convert_fusion = bf16[2,4096]{1,0:T(2,128)(2,1)} fusion(bf16[1,512,4096]{2,1,0:T(8,128)(2,1)} %param.47, bf16[2,4096]{1,0:T(2,128)(2,1)S(1)} %convolution_convert_fusion.1, bf16[1,4096,512]{2,1,0:T(8,128)(2,1)} %param.46, f32[2,512]{1,0:T(2,128)S(1)} %fusion.3, f32[2]{0:T(128)S(1)} %convolution_bitcast_fusion.5), kind=kOutput, calls=%fused_computation.4 | convolution fusion | flops 16792576 | bytes 8425480 | tf_op jit(solution)/shard_map/dot_general | solution.py:152
  158.4 3.5 %all-to-all-start.4 = ((bf16[2,16,256]{2,0,1:T(2,128)(2,1)}), bf16[2,16,256]{2,0,1:T(2,128)(2,1)S(1)}, u32[]{:S(2)}, u32[]{:S(2)}) async-start(bf16[2,16,256]{2,0,1:T(2,128)(2,1)} %bitcast.28), calls=%async_computation.4 | async-start | bytes 32768 | tf_op jit(solution)/shard_map/all_to_all | solution.py:155
  162.0 6.4 %all-to-all-done.4 = bf16[2,16,256]{2,0,1:T(2,128)(2,1)S(1)} async-done(((bf16[2,16,256]{2,0,1:T(2,128)(2,1)}), bf16[2,16,256]{2,0,1:T(2,128)(2,1)S(1)}, u32[]{:S(2)}, u32[]{:S(2)}) %all-to-all-start.4) | async-done | bytes 16416 | tf_op jit(solution)/shard_map/all_to_all | solution.py:155
  168.4 0.8 fusion.8
  (44 shorter events, 0.5 us)
Async XLA Ops:
  0.6 32.5 %copy-start = (bf16[4096,256]{1,0:T(8,128)(2,1)S(1)}, bf16[4096,256]{1,0:T(8,128)(2,1)}, u32[]{:S(2)}) copy-start(bf16[4096,256]{1,0:T(8,128)(2,1)} %param.34) | copy-start | bytes 6291460
  0.6 40.0 %copy-start.3 = (s32[8,2]{0,1:T(2,128)S(1)}, s32[8,2]{0,1:T(2,128)}, u32[]{:S(2)}) copy-start(s32[8,2]{0,1:T(2,128)} %param.42) | copy-start | bytes 196
  0.7 39.1 %copy-start.4 = (f32[8,4]{0,1:T(4,128)S(1)}, f32[8,4]{0,1:T(4,128)}, u32[]{:S(2)}) copy-start(f32[8,4]{0,1:T(4,128)} %param.43) | copy-start | bytes 388
  0.7 39.1 %copy-start.6 = (f32[8,2]{0,1:T(2,128)S(1)}, f32[8,2]{0,1:T(2,128)}, u32[]{:S(2)}) copy-start(f32[8,2]{0,1:T(2,128)} %param.44) | copy-start | bytes 196
  0.7 43.8 %copy-start.5 = (bf16[1024]{0:T(1024)(128)(2,1)S(1)}, bf16[1024]{0:T(1024)(128)(2,1)}, u32[]{:S(2)}) copy-start(bf16[1024]{0:T(1024)(128)(2,1)} %param.39) | copy-start | bytes 6148
  27.5 16.9 %all-to-all-start.1 = ((bf16[16,1,128]{2,1,0:T(2,128)(2,1)}), bf16[16,1,128]{2,1,0:T(2,128)(2,1)S(1)}, u32[]{:S(2)}, u32[]{:S(2)}) async-start(bf16[16,1,128]{2,1,0:T(2,128)(2,1)} %copy.61), calls=%async_computation.1 | async-start | bytes 16384 | tf_op jit(solution)/shard_map/all_to_all | solution.py:87
  44.5 12.3 %all-to-all-start = ((bf16[16,1,128]{2,1,0:T(2,128)(2,1)}), bf16[16,1,128]{2,1,0:T(2,128)(2,1)S(1)}, u32[]{:S(2)}, u32[]{:S(2)}) async-start(bf16[16,1,128]{2,1,0:T(2,128)(2,1)} %copy.59), calls=%async_computation | async-start | bytes 16384 | tf_op jit(solution)/shard_map/all_to_all | solution.py:86
  56.8 9.8 %all-to-all-start.2 = ((bf16[16,2,128]{2,1,0:T(2,128)(2,1)}), bf16[16,2,128]{2,1,0:T(2,128)(2,1)S(1)}, u32[]{:S(2)}, u32[]{:S(2)}) async-start(bf16[16,2,128]{2,1,0:T(2,128)(2,1)} %reshape.330), calls=%async_computation.2 | async-start | bytes 16384 | tf_op jit(solution)/shard_map/all_to_all | solution.py:88
  66.6 11.3 %all-to-all-start.3 = ((bf16[16,2,128]{2,1,0:T(2,128)(2,1)}), bf16[16,2,128]{2,1,0:T(2,128)(2,1)S(1)}, u32[]{:S(2)}, u32[]{:S(2)}) async-start(bf16[16,2,128]{2,1,0:T(2,128)(2,1)} %reshape.328), calls=%async_computation.3 | async-start | bytes 16384 | tf_op jit(solution)/shard_map/all_to_all | solution.py:89
  73.7 2.0 %copy-start.1 = (f32[2,512,1024]{2,1,0:T(8,128)}, f32[2,512,1024]{2,1,0:T(8,128)S(1)}, u32[]{:S(2)}) copy-start(f32[2,512,1024]{2,1,0:T(8,128)S(1)} %multiply_add_fusion) | copy-start | bytes 12582916
  73.8 27.0 %copy-start.2 = (bf16[8,256]{1,0:T(8,128)(2,1)S(1)}, bf16[8,256]{1,0:T(8,128)(2,1)}, u32[]{:S(2)}) copy-start(bf16[8,256]{1,0:T(8,128)(2,1)} %param.29) | copy-start | bytes 12292
  158.4 10.0 %all-to-all-start.4 = ((bf16[2,16,256]{2,0,1:T(2,128)(2,1)}), bf16[2,16,256]{2,0,1:T(2,128)(2,1)S(1)}, u32[]{:S(2)}, u32[]{:S(2)}) async-start(bf16[2,16,256]{2,0,1:T(2,128)(2,1)} %bitcast.28), calls=%async_computation.4 | async-start | bytes 32768 | tf_op jit(solution)/shard_map/all_to_all | solution.py:155
where the time goes:
time: 170 us; the launch traced here: 169 us
  blocking collectives  92.6 us (54%)
  matrix products  22.2 us (13%)
  starting transfers between devices  19.8 us (12%)
  waiting for transfers between devices  17.5 us (10%)
  other arithmetic  8.69 us (5%)
  local copies, waits for them, and re-layouts  7.43 us (4%)
    psum x1, blocking collectives, per_device(): total = lax.psum(jnp.sum(floats * floats, axis=1), 'ep')  29.8 us
    all_gather x1, blocking collectives, per_device(): rows = lax.all_gather(residual, 'ep', axis=1, tiled=True)  23.7 us
    all_gather x1, blocking collectives, per_device(): lax.all_gather(mixed, 'ep', axis=0, tiled=True)  21.8 us
    all_gather x1, blocking collectives, per_device(): lax.all_gather(scaled.astype(jnp.bfloat16), 'ep', axis=1, tiled=True)  17.3 us
    all_to_all x1, waiting for transfers between devices, per_device(): lax.all_to_all(expert_rows, 'ep', split_axis=1, concat_axis=0, tiled=True)  6.42 us
    all_to_all x1, starting transfers between devices, per_device(): lax.all_to_all(send_query, 'ep', split_axis=0, concat_axis=0, tiled=True)  5.98 us
    dot_general x4, matrix products, outgoing(): jnp.dot(picker, projected, preferred_element_type=jnp.float32)  5.92 us
    all_to_all x1, waiting for transfers between devices, per_device(): lax.all_to_all(send_value, 'ep', split_axis=0, concat_axis=0, tiled=True)  5.56 us
  transfers between devices with their start and end apart: 5, of which 3 were waited for; matrix products, arithmetic and copies ran while one was open for 12% of the time, Pallas kernels for 0%

commit v1 on v0

--- a/solution.py
+++ b/solution.py
@@ -62,7 +62,8 @@
     width = own_width * devices
     pairs_dev = head_states.shape[0]
     slot_count = max(1, pairs_dev // HEADS)
-    rows = lax.all_gather(residual, "ep", axis=1, tiled=True)
+    parts = lax.all_gather(residual, "ep", axis=0, tiled=False)
+    rows = jnp.concatenate(parts, axis=1)
     normed = rms_scale(rows, first_gain).astype(jnp.bfloat16)
     my_head = my_index * HEADS // devices
     target = jnp.arange(devices, dtype=jnp.int32)[:, None]

time: 170 us -> 168 us (0.988)
  no operation moved by 1% of the time
where the time goes in v1:
time: 168 us
  blocking collectives  92.6 us (55%)
  matrix products  20.6 us (12%)
  starting transfers between devices  19.8 us (12%)
  waiting for transfers between devices  17.5 us (10%)
  other arithmetic  8.78 us (5%)
  local copies, waits for them, and re-layouts  7.44 us (4%)
    psum x1, blocking collectives, per_device(): total = lax.psum(jnp.sum(floats * floats, axis=1), 'ep')  29.8 us
    all_gather x1, blocking collectives, per_device(): parts = lax.all_gather(residual, 'ep', axis=0, tiled=False)  23.7 us
    all_gather x1, blocking collectives, per_device(): lax.all_gather(mixed, 'ep', axis=0, tiled=True)  21.8 us
    all_gather x1, blocking collectives, per_device(): lax.all_gather(scaled.astype(jnp.bfloat16), 'ep', axis=1, tiled=True)  17.3 us
    all_to_all x1, waiting for transfers between devices, per_device(): lax.all_to_all(expert_rows, 'ep', split_axis=1, concat_axis=0, tiled=True)  6.42 us
    all_to_all x1, starting transfers between devices, per_device(): lax.all_to_all(send_query, 'ep', split_axis=0, concat_axis=0, tiled=True)  5.98 us
    all_to_all x1, waiting for transfers between devices, per_device(): lax.all_to_all(send_value, 'ep', split_axis=0, concat_axis=0, tiled=True)  5.56 us
    all_to_all x1, waiting for transfers between devices, per_device(): lax.all_to_all(send_query, 'ep', split_axis=0, concat_axis=0, tiled=True)  5.53 us
  transfers between devices with their start and end apart: 5, of which 3 were waited for; matrix products, arithmetic and copies ran while one was open for 12% of the time, Pallas kernels for 0%

profile of v1, /device:TPU:0, one launch (start us, length us, event | category | flops | bytes accessed | tf_op | source)
XLA Modules:
  0.0 167.7 jit_solution(15375977414009052667)
XLA Ops:
  0.6 0.0 copy-start
  0.6 0.0 copy-start.5
  0.8 23.7 %all-gather = bf16[128,256]{1,0:T(8,128)(2,1)S(1)} all-gather(bf16[8,256]{1,0:T(8,128)(2,1)} %param.29), channel_id=2, replica_groups=mesh['grp'=2,'ep'=16] {'ep'}, dimensions={0}, use_global_device_ids=true | all-gather | bytes 69632 | tf_op jit(solution)/shard_map/all_gather | solution.py:65
  24.5 0.1 multiply_reduce_fusion
  24.6 0.7 convert_element_type.158
  25.3 0.1 multiply_convert_fusion
  25.4 1.6 fusion.14
  27.0 0.6 copy.61
  27.6 3.4 %all-to-all-start.1 = ((bf16[16,1,128]{2,1,0:T(2,128)(2,1)}), bf16[16,1,128]{2,1,0:T(2,128)(2,1)S(1)}, u32[]{:S(2)}, u32[]{:S(2)}) async-start(bf16[16,1,128]{2,1,0:T(2,128)(2,1)} %copy.61), calls=%async_computation.1 | async-start | bytes 16384 | tf_op jit(solution)/shard_map/all_to_all | solution.py:88
  31.0 0.7 fusion.67
  31.7 0.7 fusion.70
  32.4 0.8 convert_reduce_fusion
  33.2 0.5 fusion.5
  33.7 1.1 fusion.79
  34.7 0.0 copy-done.3
  34.7 0.9 convolution_add_fusion
  35.6 0.0 copy-done.2
  35.7 0.4 fusion.13
  36.0 2.1 %fusion.6 = bf16[16,1,256]{2,0,1:T(8,128)(2,1)S(1)} fusion(bf16[8,4096]{1,0:T(8,128)(2,1)S(1)} %multiply_convert_fusion, bf16[4096,256]{1,0:T(8,128)(2,1)} %param.35, s32[16]{0:T(128)S(1)} %and_select_fusion.1, pred[16]{0:T(512)(128)(4,1)S(1)} %broadcast_compare_fusion.2), kind=kOutput, calls=%fused_computation.16 | convolution fusion | flops 16849152 | bytes 2170960 | tf_op jit(solution)/shard_map/dot_general | solution.py:79
  38.1 0.2 reduce-window.8
  38.3 0.0 copy-done.8
  38.4 0.8 dynamic-slice_convert_fusion
  39.2 0.1 convolution_bitcast_fusion.5
  39.4 0.5 broadcast.372
  39.9 0.6 reduce.7
  40.5 0.6 reshape.338
  41.1 0.6 copy.59
  41.7 0.6 reduce.6
  42.4 0.6 reshape.336
  43.0 0.0 all-to-all-done.1
  43.0 6.0 %all-to-all-start = ((bf16[16,1,128]{2,1,0:T(2,128)(2,1)}), bf16[16,1,128]{2,1,0:T(2,128)(2,1)S(1)}, u32[]{:S(2)}, u32[]{:S(2)}) async-start(bf16[16,1,128]{2,1,0:T(2,128)(2,1)} %copy.59), calls=%async_computation | async-start | bytes 16384 | tf_op jit(solution)/shard_map/all_to_all | solution.py:87
  49.0 0.2 convolution_bitcast_fusion.3
  49.2 0.6 gather_fusion.1
  49.8 5.5 %all-to-all-done = bf16[16,1,128]{2,1,0:T(2,128)(2,1)S(1)} async-done(((bf16[16,1,128]{2,1,0:T(2,128)(2,1)}), bf16[16,1,128]{2,1,0:T(2,128)(2,1)S(1)}, u32[]{:S(2)}, u32[]{:S(2)}) %all-to-all-start) | async-done | bytes 4128 | tf_op jit(solution)/shard_map/all_to_all | solution.py:87
  55.4 3.4 %all-to-all-start.2 = ((bf16[16,2,128]{2,1,0:T(2,128)(2,1)}), bf16[16,2,128]{2,1,0:T(2,128)(2,1)S(1)}, u32[]{:S(2)}, u32[]{:S(2)}) async-start(bf16[16,2,128]{2,1,0:T(2,128)(2,1)} %reshape.338), calls=%async_computation.2 | async-start | bytes 16384 | tf_op jit(solution)/shard_map/all_to_all | solution.py:89
  58.8 0.2 convolution_bitcast_fusion.4
  59.0 0.6 gather_fusion
  59.6 5.6 %all-to-all-done.2 = bf16[16,2,128]{2,1,0:T(2,128)(2,1)S(1)} async-done(((bf16[16,2,128]{2,1,0:T(2,128)(2,1)}), bf16[16,2,128]{2,1,0:T(2,128)(2,1)S(1)}, u32[]{:S(2)}, u32[]{:S(2)}) %all-to-all-start.2) | async-done | bytes 8224 | tf_op jit(solution)/shard_map/all_to_all | solution.py:89
  65.2 3.5 %all-to-all-start.3 = ((bf16[16,2,128]{2,1,0:T(2,128)(2,1)}), bf16[16,2,128]{2,1,0:T(2,128)(2,1)S(1)}, u32[]{:S(2)}, u32[]{:S(2)}) async-start(bf16[16,2,128]{2,1,0:T(2,128)(2,1)} %reshape.336), calls=%async_computation.3 | async-start | bytes 16384 | tf_op jit(solution)/shard_map/all_to_all | solution.py:90
  68.7 0.1 reduce.4
  68.7 0.2 convolution_bitcast_fusion.2
  68.9 0.6 gather_fusion.2
  69.5 2.7 %multiply_add_fusion = f32[2,512,1024]{2,1,0:T(8,128)S(1)} fusion(f32[2,512,1024]{2,1,0:T(8,128)} %param.30, f32[2,1024]{1,0:T(2,128)S(1)} %bitcast.136, f32[2,512]{1,0:T(2,128)S(1)} %bitcast.138, f32[2,512]{1,0:T(2,128)S(1)} %fusion.41), kind=kLoop, calls=%fused_computation.11 | loop fusion | flops 3145728 | bytes 8404992 | tf_op jit(solution)/shard_map/add | solution.py:117
  72.3 0.0 copy-start.1
  72.3 0.0 copy-start.4
  72.3 2.0 %copy-done.1 = f32[2,512,1024]{2,1,0:T(8,128)} copy-done((f32[2,512,1024]{2,1,0:T(8,128)}, f32[2,512,1024]{2,1,0:T(8,128)S(1)}, u32[]{:S(2)}) %copy-start.1) | copy-done | bytes 4194328
  74.3 2.1 %fusion.80 = f32[2,1,1024]{2,1,0:T(1,128)S(1)} fusion(f32[2,512,1]{1,2,0:T(1,128)S(1)} %bitcast.137, f32[2,512,1024]{2,1,0:T(8,128)S(1)} %multiply_add_fusion), kind=kOutput, calls=%fused_computation.140 | convolution fusion | flops 12582912 | bytes 4206592 | tf_op jit(solution)/shard_map/pk,pkv->pv/dot_general | solution.py:120
  76.4 0.1 fusion.29
  76.5 0.0 all-to-all-done.3
  76.5 0.1 reduce.5
  76.6 0.2 convolution_bitcast_fusion.1
  76.8 0.6 gather_fusion.3
  77.4 0.1 fusion.57
  77.5 21.8 %all-gather.1 = bf16[16,2,1024]{2,1,0:T(2,128)(2,1)S(1)} all-gather(bf16[1,2,1024]{2,1,0:T(2,128)(2,1)S(1)} %fusion.57), channel_id=1, replica_groups=mesh['grp'=2,'ep'=16] {'ep'}, dimensions={0}, use_global_device_ids=true | all-gather | bytes 69632 | tf_op jit(solution)/shard_map/all_gather | solution.py:129
  99.3 2.1 %multiply_reduce_fusion.1 = (f32[8]{0:T(128)S(1)}, f32[8,256]{1,0:T(8,128)S(1)}) fusion(bf16[8,4096]{1,0:T(8,128)(2,1)S(1)} %reshape.288, bf16[4096,256]{1,0:T(8,128)(2,1)} %param.40, bf16[8,256]{1,0:T(8,128)(2,1)S(1)} %copy-done.4), kind=kOutput, calls=%fused_computation.56 | convolution fusion | flops 16793592 | bytes 2175008 | tf_op jit(solution)/shard_map/dot_general | solution.py:130
  101.4 29.8 %psum.7 = f32[8]{0:T(128)S(1)} all-reduce(f32[8]{0:T(128)S(1)} %get-tuple-element.2), channel_id=1, replica_groups=mesh['grp'=2,'ep'=16] {'ep'}, use_global_device_ids=true, to_apply=%region_7.8 | all-reduce | flops 8 | bytes 64 | tf_op jit(solution)/shard_map/psum | solution.py:133
  131.3 0.1 multiply_convert_fusion.1
  131.3 17.3 %all_gather.15 = bf16[8,4096]{1,0:T(8,128)(2,1)S(1)} all-gather(bf16[8,256]{1,0:T(8,128)(2,1)S(1)} %multiply_convert_fusion.1), channel_id=1, replica_groups=mesh['grp'=2,'ep'=16] {'ep'}, dimensions={1}, use_global_device_ids=true | all-gather | bytes 69632 | tf_op jit(solution)/shard_map/all_gather | solution.py:136
  148.6 0.1 convolution_convert_fusion.1
  148.8 2.8 %fusion.3 = f32[2,512]{1,0:T(2,128)S(1)} fusion(bf16[2,4096]{1,0:T(2,128)(2,1)S(1)} %convolution_convert_fusion.1, bf16[1,4096,512]{2,1,0:T(8,128)(2,1)} %param.45), kind=kOutput, calls=%fused_computation.9 | convolution fusion | flops 8388608 | bytes 4214784 | tf_op jit(solution)/shard_map/dot_general | solution.py:150
  151.6 5.4 %convolution_convert_fusion = bf16[2,4096]{1,0:T(2,128)(2,1)} fusion(bf16[1,512,4096]{2,1,0:T(8,128)(2,1)} %param.47, bf16[2,4096]{1,0:T(2,128)(2,1)S(1)} %convolution_convert_fusion.1, bf16[1,4096,512]{2,1,0:T(8,128)(2,1)} %param.46, f32[2,512]{1,0:T(2,128)S(1)} %fusion.3, f32[2]{0:T(128)S(1)} %convolution_bitcast_fusion.5), kind=kOutput, calls=%fused_computation.4 | convolution fusion | flops 16792576 | bytes 8425480 | tf_op jit(solution)/shard_map/dot_general | solution.py:153
  156.9 3.5 %all-to-all-start.4 = ((bf16[2,16,256]{2,0,1:T(2,128)(2,1)}), bf16[2,16,256]{2,0,1:T(2,128)(2,1)S(1)}, u32[]{:S(2)}, u32[]{:S(2)}) async-start(bf16[2,16,256]{2,0,1:T(2,128)(2,1)} %bitcast.32), calls=%async_computation.4 | async-start | bytes 32768 | tf_op jit(solution)/shard_map/all_to_all | solution.py:156
  160.5 6.4 %all-to-all-done.4 = bf16[2,16,256]{2,0,1:T(2,128)(2,1)S(1)} async-done(((bf16[2,16,256]{2,0,1:T(2,128)(2,1)}), bf16[2,16,256]{2,0,1:T(2,128)(2,1)S(1)}, u32[]{:S(2)}, u32[]{:S(2)}) %all-to-all-start.4) | async-done | bytes 16416 | tf_op jit(solution)/shard_map/all_to_all | solution.py:156
  166.9 0.8 fusion.8
  (50 shorter events, 0.6 us)
Async XLA Ops:
  0.6 32.6 %copy-start = (bf16[4096,256]{1,0:T(8,128)(2,1)S(1)}, bf16[4096,256]{1,0:T(8,128)(2,1)}, u32[]{:S(2)}) copy-start(bf16[4096,256]{1,0:T(8,128)(2,1)} %param.34) | copy-start | bytes 6291460
  0.6 38.5 %copy-start.5 = (s32[8,2]{0,1:T(2,128)S(1)}, s32[8,2]{0,1:T(2,128)}, u32[]{:S(2)}) copy-start(s32[8,2]{0,1:T(2,128)} %param.42) | copy-start | bytes 196
  0.7 34.1 %copy-start.3 = (bf16[16,2048]{1,0:T(8,128)(2,1)S(1)}, bf16[16,2048]{1,0:T(8,128)(2,1)}, u32[]{:S(2)}) copy-start(bf16[16,2048]{1,0:T(8,128)(2,1)} %param.37) | copy-start | bytes 196612
  0.7 35.0 %copy-start.2 = (bf16[4096,128]{1,0:T(8,128)(2,1)S(1)}, bf16[4096,128]{1,0:T(8,128)(2,1)}, u32[]{:S(2)}) copy-start(bf16[4096,128]{1,0:T(8,128)(2,1)} %param.32) | copy-start | bytes 3145732
  0.7 37.6 %copy-start.6 = (f32[8,4]{0,1:T(4,128)S(1)}, f32[8,4]{0,1:T(4,128)}, u32[]{:S(2)}) copy-start(f32[8,4]{0,1:T(4,128)} %param.43) | copy-start | bytes 388
  0.7 37.6 %copy-start.8 = (f32[8,2]{0,1:T(2,128)S(1)}, f32[8,2]{0,1:T(2,128)}, u32[]{:S(2)}) copy-start(f32[8,2]{0,1:T(2,128)} %param.44) | copy-start | bytes 196
  0.7 42.3 %copy-start.7 = (bf16[1024]{0:T(1024)(128)(2,1)S(1)}, bf16[1024]{0:T(1024)(128)(2,1)}, u32[]{:S(2)}) copy-start(bf16[1024]{0:T(1024)(128)(2,1)} %param.39) | copy-start | bytes 6148
  27.6 15.4 %all-to-all-start.1 = ((bf16[16,1,128]{2,1,0:T(2,128)(2,1)}), bf16[16,1,128]{2,1,0:T(2,128)(2,1)S(1)}, u32[]{:S(2)}, u32[]{:S(2)}) async-start(bf16[16,1,128]{2,1,0:T(2,128)(2,1)} %copy.61), calls=%async_computation.1 | async-start | bytes 16384 | tf_op jit(solution)/shard_map/all_to_all | solution.py:88
  43.0 12.3 %all-to-all-start = ((bf16[16,1,128]{2,1,0:T(2,128)(2,1)}), bf16[16,1,128]{2,1,0:T(2,128)(2,1)S(1)}, u32[]{:S(2)}, u32[]{:S(2)}) async-start(bf16[16,1,128]{2,1,0:T(2,128)(2,1)} %copy.59), calls=%async_computation | async-start | bytes 16384 | tf_op jit(solution)/shard_map/all_to_all | solution.py:87
  55.4 9.8 %all-to-all-start.2 = ((bf16[16,2,128]{2,1,0:T(2,128)(2,1)}), bf16[16,2,128]{2,1,0:T(2,128)(2,1)S(1)}, u32[]{:S(2)}, u32[]{:S(2)}) async-start(bf16[16,2,128]{2,1,0:T(2,128)(2,1)} %reshape.338), calls=%async_computation.2 | async-start | bytes 16384 | tf_op jit(solution)/shard_map/all_to_all | solution.py:89
  65.2 11.3 %all-to-all-start.3 = ((bf16[16,2,128]{2,1,0:T(2,128)(2,1)}), bf16[16,2,128]{2,1,0:T(2,128)(2,1)S(1)}, u32[]{:S(2)}, u32[]{:S(2)}) async-start(bf16[16,2,128]{2,1,0:T(2,128)(2,1)} %reshape.336), calls=%async_computation.3 | async-start | bytes 16384 | tf_op jit(solution)/shard_map/all_to_all | solution.py:90
  72.3 2.0 %copy-start.1 = (f32[2,512,1024]{2,1,0:T(8,128)}, f32[2,512,1024]{2,1,0:T(8,128)S(1)}, u32[]{:S(2)}) copy-start(f32[2,512,1024]{2,1,0:T(8,128)S(1)} %multiply_add_fusion) | copy-start | bytes 12582916
  72.3 27.0 %copy-start.4 = (bf16[8,256]{1,0:T(8,128)(2,1)S(1)}, bf16[8,256]{1,0:T(8,128)(2,1)}, u32[]{:S(2)}) copy-start(bf16[8,256]{1,0:T(8,128)(2,1)} %param.29) | copy-start | bytes 12292
  156.9 10.0 %all-to-all-start.4 = ((bf16[2,16,256]{2,0,1:T(2,128)(2,1)}), bf16[2,16,256]{2,0,1:T(2,128)(2,1)S(1)}, u32[]{:S(2)}, u32[]{:S(2)}) async-start(bf16[2,16,256]{2,0,1:T(2,128)(2,1)} %bitcast.32), calls=%async_computation.4 | async-start | bytes 32768 | tf_op jit(solution)/shard_map/all_to_all | solution.py:156
